TPU v7x, 128 devices: a whole 4x4x4 slice. The times are simulated.
128 devices in a mesh: sp: 64 (over z, y, x), tp: 2 (over core).
Axes of the slice: x: 4, y: 4, z: 4, core: 2. Of those that a mesh axis runs over, the one named last changes fastest.
Arguments:
- query_rows: bfloat16 [16384, 1024], P('sp', 'tp'), may hold values from -26 to 26
- key_rows: bfloat16 [16384, 128], P('sp', 'tp'), may hold values from -26 to 26
- value_head_rows: bfloat16 [16384, 128], P('sp', 'tp'), may hold values from -6 to 6
- sink_logit_head: float32 [16], P('tp'), may hold values from -6 to 6
- out_weight: bfloat16 [1024, 2048], P('tp'), may hold values from -0.1875 to 0.1875
- residual: bfloat16 [16384, 2048], P(('sp', 'tp')), may hold values from -6 to 6
- norm_gain: float32 [2048], replicated, may hold values from 0.1 to 1.9
- routes: int32 [16384, 2], P(('sp', 'tp')), may hold values from 0 to 63, all different within a row; in each aligned block of 128 rows (0 to 127, 128 to 255, ...) at most 6 rows name the same one
- route_weights: float32 [16384, 2], P(('sp', 'tp')), may hold values from 0.1 to 1
- gate_proj: bfloat16 [64, 2048, 3584], P('sp', None, 'tp'), may hold values from -0.125 to 0.125
- up_proj: bfloat16 [64, 2048, 3584], P('sp', None, 'tp'), may hold values from -0.125 to 0.125
- down_proj: bfloat16 [64, 3584, 2048], P('sp', 'tp'), may hold values from -0.09375 to 0.09375
Outputs:
- output: bfloat16 [16384, 2048], P(('sp', 'tp'))
Inputs may be any that keep to these rules, and one draw needn't show every extreme that they name: `routes`: A row names 2 different experts. Among the rows of one device no expert is named more than 6 times, a bound that some block reaches on some devices.
All inputs are finite; a program needn't handle non-finite values.
Results may differ from a plain program's by a relative error of at most 0.0055.
Values may be sent and summed in bfloat16 or wider, within the bound.
A program may use at most 128 MiB of HBM per device.

v0:
```python
import jax
import jax.numpy as jnp
from jax import lax
from jax.sharding import PartitionSpec as P

QUERY_HEADS = 16
KEY_VALUE_HEADS = 2
HEAD_SIZE = 64
TOP = 2
WINDOW_KEYS = 128


def from_behind(block, axis, distance):
    devices = range(lax.axis_size(axis))
    route = [(i - distance, i) for i in devices if i - distance in devices]
    return lax.ppermute(block, axis, route)


def in_blocks(shard, dim, size):
    before, after = (shard.shape[:dim], shard.shape[dim + 1 :])
    return jnp.moveaxis(shard.reshape(*before, size, -1, *after), dim, 0)


def summed_on_arrival(shard, axis, dim):
    size = lax.axis_size(axis)
    tiles = lax.all_to_all(in_blocks(shard, dim, size), axis, 0, 0, tiled=True)
    return jnp.sum(tiles, axis=0)


def from_everyone(shard, axis):
    copies = jnp.broadcast_to(shard, (lax.axis_size(axis), *shard.shape))
    return lax.all_to_all(copies, axis, split_axis=0, concat_axis=0, tiled=True)


def laid_out(tiles, dim):
    dims = list(tiles.shape[1:])
    dims[dim] *= tiles.shape[0]
    return jnp.moveaxis(tiles, 0, dim).reshape(dims)


def collect(shard, axis, dim):
    tiles = from_everyone(shard, axis)
    return laid_out(tiles, dim)


def sum_at_owner(shard, axis, dim):
    tiles = in_blocks(shard, dim, lax.axis_size(axis))
    arrived = lax.all_to_all(tiles, axis, split_axis=0, concat_axis=0, tiled=True)
    return arrived.astype(jnp.float32).sum(axis=0)


def on_device(
    query_rows,
    key_rows,
    value_head_rows,
    sink_logit_head,
    out_weight,
    residual,
    norm_gain,
    routes,
    route_weights,
    gate_proj,
    up_proj,
    down_proj,
):
    length = query_rows.shape[0]
    query_group = QUERY_HEADS // KEY_VALUE_HEADS
    width = key_rows.shape[1]
    local_kv = width // HEAD_SIZE
    local_heads = local_kv * query_group
    sp_index = lax.axis_index("sp")
    tp_index = lax.axis_index("tp")
    tail = jnp.concatenate(
        [key_rows[length - WINDOW_KEYS :], value_head_rows[length - WINDOW_KEYS :]], axis=1
    )
    before = from_behind(tail, "sp", 1)
    key_all = jnp.concatenate([before[:, :width], key_rows], axis=0)
    value_all = jnp.concatenate([before[:, width:], value_head_rows], axis=0)
    score_matrix = jnp.einsum(
        "rjwh,cjh->jwrc",
        query_rows.reshape(length, local_kv, query_group, HEAD_SIZE),
        key_all.reshape(-1, local_kv, HEAD_SIZE),
        preferred_element_type=jnp.float32,
    ) * HEAD_SIZE ** (-0.5)
    query_pos = sp_index * length + jnp.arange(length, dtype=jnp.int32)
    key_pos = sp_index * length - WINDOW_KEYS + jnp.arange(length + WINDOW_KEYS, dtype=jnp.int32)
    distance = query_pos[:, None] - key_pos[None, :]
    inside = (distance >= 0) & (distance < WINDOW_KEYS) & (key_pos[None, :] >= 0)
    head_ids = (tp_index * local_heads + jnp.arange(local_heads, dtype=jnp.int32)).astype(
        jnp.float32
    )
    slope_values = jnp.exp2(-8.0 * (head_ids + 1.0) / QUERY_HEADS).reshape(local_kv, query_group)
    score_matrix = (
        score_matrix - slope_values[:, :, None, None] * distance.astype(jnp.float32)[None, None]
    )
    score_matrix = jnp.where(inside[None, None], score_matrix, -jnp.inf)
    sink_portion = sink_logit_head.reshape(local_kv, query_group)[:, :, None]
    peak = jnp.maximum(jnp.max(score_matrix, axis=-1), sink_portion)
    expd = jnp.exp(score_matrix - peak[..., None])
    denom = jnp.sum(expd, axis=-1) + jnp.exp(sink_portion - peak)
    probabilities = (expd / denom[..., None]).astype(jnp.bfloat16)
    attended = (
        jnp.einsum(
            "wfbt,twj->bwfj",
            probabilities,
            value_all.reshape(-1, local_kv, HEAD_SIZE),
            preferred_element_type=jnp.float32,
        )
        .reshape(length, local_heads * HEAD_SIZE)
        .astype(jnp.bfloat16)
    )
    own_rows = length // lax.axis_size("tp")
    projected = summed_on_arrival(
        jnp.dot(attended, out_weight, preferred_element_type=jnp.float32), "tp", 0
    )
    mixed = residual.astype(jnp.float32) + projected
    scale = lax.rsqrt(jnp.mean(mixed * mixed, axis=-1, keepdims=True) + 1e-05)
    normed = (mixed * scale * norm_gain).astype(jnp.bfloat16)
    n_sp = lax.axis_size("sp")
    n_tp = lax.axis_size("tp")
    capacity = 3 * own_rows * TOP // (2 * n_sp)
    chosen = routes.reshape(-1)
    onehot = (chosen[:, None] == jnp.arange(n_sp, dtype=jnp.int32)[None, :]).astype(jnp.int32)
    running = jnp.cumsum(onehot, axis=0)
    rank_in = jnp.sum(onehot * running, axis=1) - 1
    slot_index = chosen * capacity + rank_in
    slot_ids = jnp.arange(n_sp * capacity, dtype=jnp.int32)
    select = jnp.any(
        slot_index.reshape(own_rows, TOP)[None, :, :] == slot_ids[:, None, None], axis=-1
    )
    dispatch = jnp.dot(
        select.astype(jnp.bfloat16), normed, preferred_element_type=jnp.float32
    ).astype(jnp.bfloat16)
    model_width = dispatch.shape[1]
    landed = lax.all_to_all(
        dispatch.reshape(n_sp, capacity, model_width), "sp", split_axis=0, concat_axis=0, tiled=True
    )
    arrived = collect(landed.reshape(n_sp, 1, capacity, model_width), "tp", 1)
    rows_in = arrived.reshape(-1, model_width)
    gate = jnp.dot(rows_in, gate_proj[0], preferred_element_type=jnp.float32)
    upper = jnp.dot(rows_in, up_proj[0], preferred_element_type=jnp.float32)
    hidden = (jax.nn.silu(gate) * upper).astype(jnp.bfloat16)
    partial_out = jnp.dot(hidden, down_proj[0], preferred_element_type=jnp.float32)
    partial_out = partial_out.reshape(n_sp, n_tp, capacity, model_width)
    summed = sum_at_owner(partial_out.astype(jnp.bfloat16), "tp", 1)
    expert_out = summed.astype(jnp.bfloat16).reshape(n_sp, capacity, model_width)
    returned = lax.all_to_all(expert_out, "sp", split_axis=0, concat_axis=0, tiled=True)
    picked = returned.reshape(n_sp * capacity, model_width)[slot_index].reshape(
        own_rows, TOP, model_width
    )
    moe_sum = jnp.sum(route_weights[:, :, None] * picked.astype(jnp.float32), axis=1)
    return (mixed + moe_sum).astype(jnp.bfloat16)


def solution(mesh):
    placed = (
        P("sp", "tp"),
        P("sp", "tp"),
        P("sp", "tp"),
        P("tp"),
        P("tp", None),
        P(("sp", "tp"), None),
        P(),
        P(("sp", "tp"), None),
        P(("sp", "tp"), None),
        P("sp", None, "tp"),
        P("sp", None, "tp"),
        P("sp", "tp", None),
    )
    return jax.shard_map(
        on_device, mesh=mesh, in_specs=placed, out_specs=P(("sp", "tp"), None), check_vma=False
    )
```

profile of v0, /device:TPU:0, one launch (start us, length us, event | category | flops | bytes accessed | tf_op | source)
XLA Modules:
  0.0 179.4 jit_solution(1945133649310377848)
XLA Ops:
  0.0 0.9 slice.18
  0.9 0.7 slice.19
  1.6 3.5 %collective-permute-start = (bf16[128,128]{0,1:T(8,128)(2,1)S(1)}, bf16[128,128]{0,1:T(8,128)(2,1)S(1)}, u32[]{:S(2)}, u32[]{:S(2)}) collective-permute-start(bf16[128,128]{0,1:T(8,128)(2,1)S(1)} %pad_maximum_fusion), channel_id=1, source_target_pairs={{0,2},{2,4},{4,6},{6,8},{8,10},{10,12},{12,14},{14,16},{16,18},{18... | collective-permute-start | bytes 98312 | tf_op jit(solution)/shard_map/ppermute | solution.py:16
  5.1 0.8 copy.60
  6.6 0.6 reduce-window.6
  7.8 1.1 copy.56
  9.0 1.5 fusion.44
  11.1 0.7 fusion.24
  11.9 0.7 fusion.17
  12.6 5.4 %all_to_all.25 = f32[2,128,2048]{2,1,0:T(8,128)S(1)} all-to-all(f32[2,128,2048]{2,1,0:T(8,128)S(1)} %fusion.17), channel_id=1, replica_groups=mesh['sp'=64,'tp'=2] {'tp'}, dimensions={0} | all-to-all | bytes 4194304 | tf_op jit(solution)/shard_map/all_to_all | solution.py:26
  18.3 1.3 multiply_reduce_fusion.1
  19.6 2.8 %convolution_convert_fusion = bf16[384,2048]{1,0:T(8,128)(2,1)} fusion(pred[384,128]{1,0:T(8,128)(4,1)S(1)} %fusion.29, f32[2048]{0:T(1024)S(1)} %copy-done.4, f32[128]{0:T(128)S(1)} %add_rsqrt_fusion, f32[128,2048]{1,0:T(8,128)S(1)} %reduce_sum.58, bf16[128,2048]{1,0:T(8,128)(2,1)} %param.17), kind=kOutput, calls=%fused_computation.15 | convolution fusion | flops 203423744 | bytes 3203584 | tf_op jit(solution)/shard_map/dot_general | solution.py:131
  22.4 2.5 %reshape.282 = bf16[64,6,2048]{2,1,0:T(8,128)(2,1)S(1)} reshape(bf16[384,2048]{1,0:T(8,128)(2,1)} %convolution_convert_fusion) | data formatting | bytes 3145728 | tf_op jit(solution)/shard_map/reshape | solution.py:136
  24.9 41.3 %all_to_all.26 = bf16[64,6,2048]{2,1,0:T(8,128)(2,1)S(1)} all-to-all(bf16[64,6,2048]{2,1,0:T(8,128)(2,1)S(1)} %reshape.282), channel_id=1, replica_groups=mesh['sp'=64,'tp'=2] {'sp'}, dimensions={0} | all-to-all | bytes 3145728 | tf_op jit(solution)/shard_map/all_to_all | solution.py:135
  66.2 0.9 copy.65
  67.5 6.3 %all_to_all.27 = bf16[2,64,1,6,2048]{4,1,3,2,0:T(8,128)(2,1)S(1)} all-to-all(bf16[2,64,1,6,2048]{4,1,3,2,0:T(8,128)(2,1)S(1)} %broadcast_in_dim.16), channel_id=1, replica_groups=mesh['sp'=64,'tp'=2] {'tp'}, dimensions={0} | all-to-all | bytes 6291456 | tf_op jit(solution)/shard_map/all_to_all | solution.py:32
  73.8 3.7 %copy.66 = bf16[64,2,1,6,2048]{4,3,1,0,2:T(8,128)(2,1)} copy(bf16[64,2,1,6,2048]{4,0,3,2,1:T(8,128)(2,1)S(1)} %bitcast.84) | data formatting | bytes 6291456 | tf_op jit(solution)/shard_map/transpose | solution.py:38
  77.4 6.3 %reshape_reshape.3 = bf16[768,2048]{1,0:T(8,128)(2,1)} reshape(bf16[64,2,1,6,2048]{4,3,1,0,2:T(8,128)(2,1)} %copy.66) | data formatting | bytes 6291456 | tf_op jit(solution)/shard_map/reshape;reshape | solution.py:139
  83.8 10.0 %fusion.4 = f32[768,1792]{1,0:T(8,128)S(1)} fusion(bf16[768,2048]{1,0:T(8,128)(2,1)} %reshape_reshape.3, bf16[1,2048,1792]{2,1,0:T(8,128)(2,1)} %param.21), kind=kOutput, calls=%fused_computation.5 | convolution fusion | flops 5637144576 | bytes 15990784 | tf_op jit(solution)/shard_map/dot_general | solution.py:140
  93.8 10.6 %multiply_convert_fusion = bf16[768,1792]{1,0:T(8,128)(2,1)} fusion(f32[768,1792]{1,0:T(8,128)S(1)} %fusion.4, bf16[768,2048]{1,0:T(8,128)(2,1)S(1)} %copy-done.3, bf16[1,2048,1792]{2,1,0:T(8,128)(2,1)} %param.22), kind=kOutput, calls=%fused_computation.7 | convolution fusion | flops 5645402112 | bytes 18743296 | tf_op jit(solution)/shard_map/dot_general | solution.py:141
  104.4 5.4 %dot_general.29 = bf16[64,2,6,1792]{3,2,1,0:T(8,128)(2,1)} reshape(bf16[768,1792]{1,0:T(8,128)(2,1)} %multiply_convert_fusion) | data formatting | bytes 5505024 | tf_op jit(solution)/shard_map/dot_general | solution.py:143
  109.8 9.8 %fusion.12 = bf16[2,64,1,6,2048]{4,1,3,2,0:T(8,128)(2,1)S(1)} fusion(bf16[1,1792,2048]{2,1,0:T(8,128)(2,1)} %param.23, bf16[64,2,6,1792]{3,2,1,0:T(8,128)(2,1)} %dot_general.29), kind=kOutput, calls=%fused_computation.14 | convolution fusion | flops 5638717440 | bytes 13238272 | tf_op jit(solution)/shard_map/dot_general | solution.py:143
  119.7 6.3 %all_to_all.28 = bf16[2,64,1,6,2048]{4,1,3,2,0:T(8,128)(2,1)S(1)} all-to-all(bf16[2,64,1,6,2048]{4,1,3,2,0:T(8,128)(2,1)S(1)} %fusion.12), channel_id=1, replica_groups=mesh['sp'=64,'tp'=2] {'tp'}, dimensions={0} | all-to-all | bytes 6291456 | tf_op jit(solution)/shard_map/all_to_all | solution.py:48
  125.9 0.7 bitcast_reduce_fusion
  126.6 2.2 %copy.70 = bf16[64,6,2048]{2,1,0:T(8,128)(2,1)} copy(bf16[64,6,2048]{2,0,1:T(8,128)(2,1)S(1)} %bitcast_reduce_fusion) | data formatting | bytes 3145728 | tf_op jit(solution)/shard_map/reduce_sum | solution.py:49
  128.8 5.9 %all-to-all-start.4 = ((bf16[64,6,2048]{2,1,0:T(8,128)(2,1)}), bf16[64,6,2048]{2,1,0:T(8,128)(2,1)}, u32[]{:S(2)}, u32[]{:S(2)}) async-start(bf16[64,6,2048]{2,1,0:T(8,128)(2,1)} %copy.70), calls=%async_computation.4 | async-start | bytes 4194304 | tf_op jit(solution)/shard_map/all_to_all | solution.py:147
  135.0 30.0 %all-to-all-done.4 = bf16[64,6,2048]{2,1,0:T(8,128)(2,1)} async-done(((bf16[64,6,2048]{2,1,0:T(8,128)(2,1)}), bf16[64,6,2048]{2,1,0:T(8,128)(2,1)}, u32[]{:S(2)}, u32[]{:S(2)}) %all-to-all-start.4) | async-done | bytes 1572896 | tf_op jit(solution)/shard_map/all_to_all | solution.py:147
  165.1 2.6 %reshape.284 = bf16[384,2048]{1,0:T(8,128)(2,1)S(1)} reshape(bf16[64,6,2048]{2,1,0:T(8,128)(2,1)} %all-to-all-done.4) | data formatting | bytes 3145728 | tf_op jit(solution)/shard_map/reshape | solution.py:148
  167.7 2.3 %gather_fusion = bf16[256,2048]{1,0:T(8,128)(2,1)} fusion(bf16[384,2048]{1,0:T(8,128)(2,1)S(1)} %reshape.284, s32[1024]{0:T(1024)S(1)} %pad_clamp_fusion), kind=kCustom, calls=%fused_computation | custom fusion | bytes 2098176 | tf_op jit(solution)/shard_map/gather | solution.py:148
  170.0 3.5 %reshape.285 = f32[128,2,2048]{2,1,0:T(2,128)} reshape(bf16[256,2048]{1,0:T(8,128)(2,1)} %gather_fusion) | data formatting | bytes 3145728 | tf_op jit(solution)/shard_map/convert_element_type | solution.py:151
  173.6 4.9 %multiply_reduce_fusion = f32[128,2048]{1,0:T(8,128)S(1)} fusion(f32[128,2,2048]{2,1,0:T(2,128)} %reshape.285, f32[128,2]{1,0:T(8,128)S(1)} %copy.59), kind=kLoop, calls=%fused_computation.20 | loop fusion | flops 786432 | bytes 3146752 | tf_op jit(solution)/shard_map/reduce_sum | solution.py:151
  178.5 1.0 add_convert_fusion
  (48 shorter events, 2.8 us)
Async XLA Ops:
  0.0 11.9 %copy-start = (bf16[512,2048]{1,0:T(8,128)(2,1)S(1)}, bf16[512,2048]{1,0:T(8,128)(2,1)}, u32[]{:S(2)}) copy-start(bf16[512,2048]{1,0:T(8,128)(2,1)} %param.16) | copy-start | bytes 6291460
  1.6 7.3 %collective-permute-start = (bf16[128,128]{0,1:T(8,128)(2,1)S(1)}, bf16[128,128]{0,1:T(8,128)(2,1)S(1)}, u32[]{:S(2)}, u32[]{:S(2)}) collective-permute-start(bf16[128,128]{0,1:T(8,128)(2,1)S(1)} %pad_maximum_fusion), channel_id=1, source_target_pairs={{0,2},{2,4},{4,6},{6,8},{8,10},{10,12},{12,14},{14,16},{16,18},{18... | collective-permute-start | bytes 98312 | tf_op jit(solution)/shard_map/ppermute | solution.py:16
  6.5 4.0 %copy-start.6 = (f32[8]{0:T(128)S(1)}, f32[8]{0:T(128)}, u32[]{:S(2)}) copy-start(f32[8]{0:T(128)} %param.15) | copy-start | bytes 100
  8.9 2.2 %copy-start.5 = (bf16[256,64]{0,1:T(8,128)(2,1)S(1)}, bf16[256,64]{0,1:T(8,128)(2,1)}, u32[]{:S(2)}) copy-start(bf16[256,64]{0,1:T(8,128)(2,1)} %param.14) | copy-start | bytes 98308
  18.1 1.5 copy-start.4
  83.8 10.0 %copy-start.3 = (bf16[768,2048]{1,0:T(8,128)(2,1)S(1)}, bf16[768,2048]{1,0:T(8,128)(2,1)}, u32[]{:S(2)}) copy-start(bf16[768,2048]{1,0:T(8,128)(2,1)} %reshape_reshape.3) | copy-start | bytes 9437188
  126.6 8.3 %copy-start.7 = (f32[128,2]{0,1:T(2,128)S(1)}, f32[128,2]{0,1:T(2,128)}, u32[]{:S(2)}) copy-start(f32[128,2]{0,1:T(2,128)} %param.20) | copy-start | bytes 3076
  128.8 36.3 %all-to-all-start.4 = ((bf16[64,6,2048]{2,1,0:T(8,128)(2,1)}), bf16[64,6,2048]{2,1,0:T(8,128)(2,1)}, u32[]{:S(2)}, u32[]{:S(2)}) async-start(bf16[64,6,2048]{2,1,0:T(8,128)(2,1)} %copy.70), calls=%async_computation.4 | async-start | bytes 4194304 | tf_op jit(solution)/shard_map/all_to_all | solution.py:147
  170.0 9.4 %copy-start.1 = (bf16[512,2048]{1,0:T(8,128)(2,1)S(1)}, bf16[512,2048]{1,0:T(8,128)(2,1)}, u32[]{:S(2)}) copy-start(bf16[512,2048]{1,0:T(8,128)(2,1)} %param.16) | copy-start | bytes 6291460
  173.6 4.9 %copy-start.2 = (bf16[128,2048]{1,0:T(8,128)(2,1)S(1)}, bf16[128,2048]{1,0:T(8,128)(2,1)}, u32[]{:S(2)}) copy-start(bf16[128,2048]{1,0:T(8,128)(2,1)} %param.17) | copy-start | bytes 1572868
where the time goes:
time: 180 us; the launch traced here: 179 us
  blocking collectives  59.3 us (33%)
  matrix products  36.3 us (20%)
  local copies, waits for them, and re-layouts  34.3 us (19%)
  waiting for transfers between devices  30 us (17%)
  other arithmetic  9.79 us (5%)
  starting transfers between devices  9.44 us (5%)
    all_to_all x1, blocking collectives, on_device(): lax.all_to_all(dispatch.reshape(n_sp, capacity, model_width), 'sp', split...  41.3 us
    all_to_all x1, waiting for transfers between devices, on_device(): lax.all_to_all(expert_out, 'sp', split_axis=0, concat_axis=0, tiled=True)  30 us
    dot_general x1, matrix products, on_device(): upper = jnp.dot(rows_in, up_proj[0], preferred_element_type=jnp.float32)  10.6 us
    dot_general x1, matrix products, on_device(): gate = jnp.dot(rows_in, gate_proj[0], preferred_element_type=jnp.float32)  10 us
    dot_general x1, matrix products, on_device(): jnp.dot(hidden, down_proj[0], preferred_element_type=jnp.float32)  9.82 us
    another operation x1, local copies, waits for them, and re-layouts, on_device(): rows_in = arrived.reshape(-1, model_width)  6.33 us
    all_to_all x1, blocking collectives, from_everyone(): return lax.all_to_all(copies, axis, split_axis=0, concat_axis=0, tiled=True)  6.26 us
    all_to_all x1, blocking collectives, sum_at_owner(): lax.all_to_all(tiles, axis, split_axis=0, concat_axis=0, tiled=True)  6.26 us
  transfers between devices with their start and end apart: 2, of which 1 were waited for; matrix products, arithmetic and copies ran while one was open for 2% of the time, Pallas kernels for 0%

commit v1 on v0

v1 whole, which is shorter than its diff:
```python
import functools

import jax
import jax.numpy as jnp
from jax import lax
from jax.experimental import pallas as pl
from jax.experimental.pallas import tpu as pltpu
from jax.sharding import PartitionSpec as P

QUERY_HEADS = 16
KEY_VALUE_HEADS = 2
HEAD_SIZE = 64
TOP = 2
WINDOW_KEYS = 128

MESH = pl.DeviceIdType.MESH
F32 = jnp.float32
BF16 = jnp.bfloat16

ROWS = 128
D = 2048
FFH = 1792
CAP = 6
Q = 4
W = D // Q
BLK = Q * CAP
CH = 4
PER = 16
GB = 8
GR = GB * CAP


def from_behind(block, axis, distance):
    devices = range(lax.axis_size(axis))
    route = [(i - distance, i) for i in devices if i - distance in devices]
    return lax.ppermute(block, axis, route)


def in_blocks(shard, dim, size):
    before, after = (shard.shape[:dim], shard.shape[dim + 1 :])
    return jnp.moveaxis(shard.reshape(*before, size, -1, *after), dim, 0)


def summed_on_arrival(shard, axis, dim):
    size = lax.axis_size(axis)
    tiles = lax.all_to_all(in_blocks(shard, dim, size), axis, 0, 0, tiled=True)
    return jnp.sum(tiles, axis=0)


def fiota(shape, dim):
    return lax.broadcasted_iota(jnp.int32, shape, dim).astype(F32)


def fdiv(v, n):
    return jnp.floor((v + 0.5) * (1.0 / n))


def offset_of(g, i):
    dz = i % 4
    dy = (i // 4 + i) % 4
    dx = (g + 8 - dz - dy) % 4
    return dx, dy, dz


def block_facts(g, r, x, y, z):
    i = fdiv(r, BLK)
    rest = r - i * BLK
    q = fdiv(rest, CAP)
    s = rest - q * CAP
    hi = fdiv(i, 4)
    dz = i - hi * 4
    dy = (hi + dz) - 4.0 * fdiv(hi + dz, 4)
    dx = (g + 8 - dz - dy) - 4.0 * fdiv(g + 8 - dz - dy, 4)
    ex = (x + dx) - 4.0 * fdiv(x + dx, 4)
    ey = (y + dy) - 4.0 * fdiv(y + dy, 4)
    ez = (z + dz) - 4.0 * fdiv(z + dz, 4)
    return ez * 16 + ey * 4 + ex, q, s


def moe_kernel(
    mixed_ref,
    gain_ref,
    routes_ref,
    rw_ref,
    wg_hbm,
    wu_hbm,
    wd_hbm,
    out_ref,
    wg,
    wu,
    wd,
    nrm,
    sbuf,
    mine,
    other,
    xbuf,
    hid,
    pm,
    po,
    pr,
    ysend,
    zbuf,
    acc,
    wsem,
    dsend,
    drecv,
    fsend,
    frecv,
    psend,
    precv,
    rsend,
    rrecv,
):
    sp = lax.axis_index("sp")
    tp = lax.axis_index("tp")
    x, y, z = sp % 4, (sp // 4) % 4, sp // 16
    partner = (sp, 1 - tp)

    wcopies = []
    for k, (src, dst) in enumerate(((wg_hbm, wg), (wu_hbm, wu), (wd_hbm, wd))):
        part = src.shape[1] // 4
        for j in range(4):
            rows = pl.ds(j * part, part)
            wcopies.append(pltpu.make_async_copy(src.at[0, rows], dst.at[rows], wsem.at[k, j]))
    for c in wcopies:
        c.start()

    barrier = pltpu.get_barrier_semaphore()

    def greet(i, _):
        pl.semaphore_signal(barrier, inc=1, device_id=((sp + i) % 64, tp), device_id_type=MESH)
        return 0

    lax.fori_loop(1, 64, greet, 0)
    pl.semaphore_signal(barrier, inc=1, device_id=partner, device_id_type=MESH)

    m = mixed_ref[...]
    scale = lax.rsqrt(jnp.mean(m * m, axis=-1, keepdims=True) + 1e-05)
    n = (m * scale * gain_ref[...]).astype(BF16)
    for q in range(Q):
        nrm[q * ROWS : (q + 1) * ROWS, :] = n[:, q * W : (q + 1) * W]
        acc[q * ROWS : (q + 1) * ROWS, :] = m[:, q * W : (q + 1) * W]

    xf, yf, zf = x.astype(F32), y.astype(F32), z.astype(F32)
    routes = routes_ref[...].astype(F32)
    r0c = jnp.broadcast_to(routes[:, 0:1], (ROWS, ROWS))
    r1c = jnp.broadcast_to(routes[:, 1:2], (ROWS, ROWS))
    ri, ci = fiota((ROWS, ROWS), 0), fiota((ROWS, ROWS), 1)
    eye = jnp.where(ri == ci, 1.0, 0.0)
    r0 = jnp.sum(r0c * eye, axis=0, keepdims=True)
    r1 = jnp.sum(r1c * eye, axis=0, keepdims=True)
    upper = jnp.where(ri < ci, 1.0, 0.0).astype(BF16)
    lower = jnp.where(ci < ri, 1.0, 0.0).astype(BF16)

    def build(g):
        e, q, s = block_facts(g, fiota((PER * BLK, ROWS), 0), xf, yf, zf)
        cnt = jnp.where((e == r0) | (e == r1), 1.0, 0.0)
        rank = jnp.dot(cnt.astype(BF16), upper, preferred_element_type=F32)
        sel = jnp.where(rank == s, cnt, 0.0)
        parts = [jnp.where(q == k, sel, 0.0).astype(BF16) for k in range(Q)]
        onehot = jnp.concatenate(parts, axis=1)
        rows = jnp.dot(onehot, nrm[...], preferred_element_type=F32).astype(BF16)
        rows = rows.reshape(PER, BLK, W)
        sbuf[pl.ds(g * PER, PER)] = rows
        if g == 0:
            mine[0] = rows[0]

    def lo_of(g):
        return 1 if g == 0 else 0

    def exchange(g, src, dst, ssem, rsem, sign):
        def one(i, _):
            dx, dy, dz = offset_of(g, i)
            peer = (
                ((z + sign * dz + 4) % 4) * 16
                + ((y + sign * dy + 4) % 4) * 4
                + (x + sign * dx + 4) % 4
            )
            pltpu.make_async_remote_copy(
                src_ref=src.at[g * PER + i],
                dst_ref=dst.at[g * PER + i],
                send_sem=ssem.at[g],
                recv_sem=rsem.at[g],
                device_id=(peer, tp),
                device_id_type=MESH,
            ).start()
            return 0

        lax.fori_loop(lo_of(g), PER, one, 0)

    def whole(g, src, dst, ssem, rsem):
        rows = pl.ds(g * PER + lo_of(g), PER - lo_of(g))
        return pltpu.make_async_remote_copy(
            src_ref=src.at[rows],
            dst_ref=dst.at[rows],
            send_sem=ssem.at[g],
            recv_sem=rsem.at[g],
            device_id=partner,
            device_id_type=MESH,
        )

    def forward(g):
        rows = pl.ds(g * PER, PER)
        return pltpu.make_async_remote_copy(
            src_ref=mine.at[rows],
            dst_ref=other.at[rows],
            send_sem=fsend.at[g],
            recv_sem=frecv.at[g],
            device_id=partner,
            device_id_type=MESH,
        )

    def swap(g):
        return pltpu.make_async_remote_copy(
            src_ref=po.at[g],
            dst_ref=pr.at[g],
            send_sem=psend.at[g],
            recv_sem=precv.at[g],
            device_id=partner,
            device_id_type=MESH,
        )

    build(0)
    pl.semaphore_wait(barrier, 64)
    exchange(0, sbuf, mine, dsend, drecv, 1)
    for g in range(1, CH):
        build(g)
        exchange(g, sbuf, mine, dsend, drecv, 1)

    pi, pj = fiota((GB * BLK, GB * BLK), 0), fiota((GB * BLK, GB * BLK), 1)
    iq = fdiv(pi, GR)
    ib = fdiv(pi - iq * GR, CAP)
    ist = pi - iq * GR - ib * CAP
    unpack = jnp.where(ib * BLK + iq * CAP + ist == pj, 1.0, 0.0).astype(BF16)
    jq = fdiv(pj, GR)
    jb = fdiv(pj - jq * GR, CAP)
    js = pj - jq * GR - jb * CAP
    pack = jnp.where(jb * BLK + jq * CAP + js == pi, 1.0, 0.0).astype(BF16)

    def spread(g):
        for h in range(4):
            src = mine if h < 2 else other
            blocks = src[pl.ds(g * PER + (h % 2) * GB, GB)].reshape(GB * BLK, W)
            rows = jnp.dot(unpack, blocks, preferred_element_type=F32).astype(BF16)
            for q in range(Q):
                xbuf[h * GR : (h + 1) * GR, q * W : (q + 1) * W] = rows[q * GR : (q + 1) * GR]

    def gate_up():
        def tile(k, _):
            cols = pl.ds(pl.multiple_of(k * 256, 256), 256)
            a = jnp.dot(xbuf[...], wg[:, cols], preferred_element_type=F32)
            b = jnp.dot(xbuf[...], wu[:, cols], preferred_element_type=F32)
            hid[:, cols] = (a / (1.0 + jnp.exp(-a)) * b).astype(BF16)
            return 0

        lax.fori_loop(0, FFH // 256, tile, 0)

    def down(g):
        def tile(k, _):
            cols = pl.ds(pl.multiple_of(k * 512, 512), 512)
            a = jnp.dot(hid[...], wd[:, cols], preferred_element_type=F32).astype(BF16)
            pm[:, cols] = a[: 2 * GR]
            po[g, :, cols] = a[2 * GR :]
            return 0

        lax.fori_loop(0, D // 512, tile, 0)

    def give_back(g):
        swap(g).wait_recv()
        for h in range(2):
            rows = slice(h * GR, (h + 1) * GR)
            total = (pm[rows].astype(F32) + pr[g, rows].astype(F32)).astype(BF16)
            stack = jnp.concatenate([total[:, q * W : (q + 1) * W] for q in range(Q)], axis=0)
            packed = jnp.dot(pack, stack, preferred_element_type=F32).astype(BF16)
            packed = packed.reshape(GB, BLK, W)
            ysend[pl.ds(g * PER + h * GB, GB)] = packed
            if g == 0 and h == 0:
                zbuf[0] = packed[0]
        exchange(g, ysend, zbuf, rsend, rrecv, -1)

    whole(0, sbuf, mine, dsend, drecv).wait_recv()
    forward(0).start()
    for c in wcopies:
        c.wait()
    for g in range(CH):
        forward(g).wait_recv()
        spread(g)
        if g > 0:
            give_back(g - 1)
        gate_up()
        if g + 1 < CH:
            whole(g + 1, sbuf, mine, dsend, drecv).wait_recv()
            forward(g + 1).start()
        down(g)
        swap(g).start()
    give_back(CH - 1)

    w0, w1 = rw_ref[:, 0:1], rw_ref[:, 1:2]
    c0, c1 = routes[:, 0:1], routes[:, 1:2]
    for g in range(CH):
        e, q, s = block_facts(g, fiota((ROWS, PER * BLK), 1), xf, yf, zf)
        is0, is1 = e == c0, e == c1
        cnt = jnp.where(is0 | is1, 1.0, 0.0)
        rank = jnp.dot(lower, cnt.astype(BF16), preferred_element_type=F32)
        wt = jnp.where(is0, w0, 0.0) + jnp.where(is1, w1, 0.0)
        wt = jnp.where(rank == s, wt, 0.0)
        whi = wt.astype(BF16)
        wlo = (wt - whi.astype(F32)).astype(BF16)
        whole(g, ysend, zbuf, rsend, rrecv).wait_recv()
        back = zbuf[pl.ds(g * PER, PER)].reshape(PER * BLK, W)
        for k in range(Q):
            here = q == k
            hi = jnp.where(here, whi.astype(F32), 0.0).astype(BF16)
            lo = jnp.where(here, wlo.astype(F32), 0.0).astype(BF16)
            both = jnp.dot(hi, back, preferred_element_type=F32) + jnp.dot(
                lo, back, preferred_element_type=F32
            )
            rows = slice(k * ROWS, (k + 1) * ROWS)
            if g + 1 < CH:
                acc[rows] += both
            else:
                out_ref[:, k * W : (k + 1) * W] = (acc[rows] + both).astype(BF16)

    for g in range(CH):
        whole(g, sbuf, mine, dsend, drecv).wait_send()
        forward(g).wait_send()
        swap(g).wait_send()
        whole(g, ysend, zbuf, rsend, rrecv).wait_send()


def moe(mixed, gain, routes, route_weights, gate_proj, up_proj, down_proj):
    vm = pl.BlockSpec(memory_space=pltpu.VMEM)
    hbm = pl.BlockSpec(memory_space=pl.ANY)
    sem = pltpu.SemaphoreType.DMA
    return pl.pallas_call(
        moe_kernel,
        out_shape=jax.ShapeDtypeStruct((ROWS, D), BF16),
        in_specs=[vm, vm, vm, vm, hbm, hbm, hbm],
        out_specs=vm,
        scratch_shapes=[
            pltpu.VMEM((D, FFH), BF16),
            pltpu.VMEM((D, FFH), BF16),
            pltpu.VMEM((FFH, D), BF16),
            pltpu.VMEM((Q * ROWS, W), BF16),
            pltpu.VMEM((CH * PER, BLK, W), BF16),
            pltpu.VMEM((CH * PER, BLK, W), BF16),
            pltpu.VMEM((CH * PER, BLK, W), BF16),
            pltpu.VMEM((4 * GR, D), BF16),
            pltpu.VMEM((4 * GR, FFH), BF16),
            pltpu.VMEM((2 * GR, D), BF16),
            pltpu.VMEM((CH, 2 * GR, D), BF16),
            pltpu.VMEM((CH, 2 * GR, D), BF16),
            pltpu.VMEM((CH * PER, BLK, W), BF16),
            pltpu.VMEM((CH * PER, BLK, W), BF16),
            pltpu.VMEM((Q * ROWS, W), F32),
            sem((3, 4)),
            sem((CH,)),
            sem((CH,)),
            sem((CH,)),
            sem((CH,)),
            sem((CH,)),
            sem((CH,)),
            sem((CH,)),
            sem((CH,)),
        ],
        compiler_params=pltpu.CompilerParams(
            collective_id=0, has_side_effects=True, vmem_limit_bytes=60 * 1024 * 1024
        ),
        name="moe",
    )(mixed, gain.reshape(1, D), routes, route_weights, gate_proj, up_proj, down_proj)


def on_device(
    query_rows,
    key_rows,
    value_head_rows,
    sink_logit_head,
    out_weight,
    residual,
    norm_gain,
    routes,
    route_weights,
    gate_proj,
    up_proj,
    down_proj,
):
    length = query_rows.shape[0]
    query_group = QUERY_HEADS // KEY_VALUE_HEADS
    width = key_rows.shape[1]
    local_kv = width // HEAD_SIZE
    local_heads = local_kv * query_group
    sp_index = lax.axis_index("sp")
    tp_index = lax.axis_index("tp")
    tail = jnp.concatenate(
        [key_rows[length - WINDOW_KEYS :], value_head_rows[length - WINDOW_KEYS :]], axis=1
    )
    before = from_behind(tail, "sp", 1)
    key_all = jnp.concatenate([before[:, :width], key_rows], axis=0)
    value_all = jnp.concatenate([before[:, width:], value_head_rows], axis=0)
    score_matrix = jnp.einsum(
        "rjwh,cjh->jwrc",
        query_rows.reshape(length, local_kv, query_group, HEAD_SIZE),
        key_all.reshape(-1, local_kv, HEAD_SIZE),
        preferred_element_type=jnp.float32,
    ) * HEAD_SIZE ** (-0.5)
    query_pos = sp_index * length + jnp.arange(length, dtype=jnp.int32)
    key_pos = sp_index * length - WINDOW_KEYS + jnp.arange(length + WINDOW_KEYS, dtype=jnp.int32)
    distance = query_pos[:, None] - key_pos[None, :]
    inside = (distance >= 0) & (distance < WINDOW_KEYS) & (key_pos[None, :] >= 0)
    head_ids = (tp_index * local_heads + jnp.arange(local_heads, dtype=jnp.int32)).astype(
        jnp.float32
    )
    slope_values = jnp.exp2(-8.0 * (head_ids + 1.0) / QUERY_HEADS).reshape(local_kv, query_group)
    score_matrix = (
        score_matrix - slope_values[:, :, None, None] * distance.astype(jnp.float32)[None, None]
    )
    score_matrix = jnp.where(inside[None, None], score_matrix, -jnp.inf)
    sink_portion = sink_logit_head.reshape(local_kv, query_group)[:, :, None]
    peak = jnp.maximum(jnp.max(score_matrix, axis=-1), sink_portion)
    expd = jnp.exp(score_matrix - peak[..., None])
    denom = jnp.sum(expd, axis=-1) + jnp.exp(sink_portion - peak)
    probabilities = (expd / denom[..., None]).astype(jnp.bfloat16)
    attended = (
        jnp.einsum(
            "wfbt,twj->bwfj",
            probabilities,
            value_all.reshape(-1, local_kv, HEAD_SIZE),
            preferred_element_type=jnp.float32,
        )
        .reshape(length, local_heads * HEAD_SIZE)
        .astype(jnp.bfloat16)
    )
    projected = summed_on_arrival(
        jnp.dot(attended, out_weight, preferred_element_type=jnp.float32), "tp", 0
    )
    mixed = residual.astype(jnp.float32) + projected
    return moe(mixed, norm_gain, routes, route_weights, gate_proj, up_proj, down_proj)


def solution(mesh):
    placed = (
        P("sp", "tp"),
        P("sp", "tp"),
        P("sp", "tp"),
        P("tp"),
        P("tp", None),
        P(("sp", "tp"), None),
        P(),
        P(("sp", "tp"), None),
        P(("sp", "tp"), None),
        P("sp", None, "tp"),
        P("sp", None, "tp"),
        P("sp", "tp", None),
    )
    return jax.shard_map(
        on_device, mesh=mesh, in_specs=placed, out_specs=P(("sp", "tp"), None), check_vma=False
    )
```

time: 180 us -> 94.1 us (0.52)
  Pallas kernels: 0 us -> 68.4 us
  blocking collectives: 59.3 us -> 6.31 us
  matrix products: 36.3 us -> 2.97 us
  waiting for transfers between devices: 30 us -> 0.01 us
  local copies, waits for them, and re-layouts: 34.3 us -> 7.46 us
  starting transfers between devices: 9.44 us -> 3.5 us
  other arithmetic: 9.79 us -> 4.89 us
    pallas_call x0 -> x1, Pallas kernels: none -> 68.4 us  [moe(): pl.pallas_call(moe_kernel, out_shape=jax.ShapeDtypeStruct((ROWS, D), BF16...]
    all_to_all x3 -> x0, blocking collectives: 53.8 us -> none  [the longest x1 41.3 us: on_device(): lax.all_to_all(dispatch.reshape(n_sp, capacity, model_width), 'sp', split...]
    dot_general x4 -> x0, matrix products: 33.3 us -> none  [the longest x1 10.6 us: on_device(): upper = jnp.dot(rows_in, up_proj[0], preferred_element_type=jnp.float32)]
    all_to_all x1 -> x0, waiting for transfers between devices: 30 us -> none  [on_device(): lax.all_to_all(expert_out, 'sp', split_axis=0, concat_axis=0, tiled=True)]
    reduce_sum x4 -> x0, other arithmetic: 6.9 us -> none  [the longest x1 4.86 us: on_device(): jnp.sum(route_weights[:, :, None] * picked.astype(jnp.float32), axis=1)]
    another operation x2 -> x0, local copies, waits for them, and re-layouts: 6.34 us -> none  [the longest x1 6.33 us: on_device(): rows_in = arrived.reshape(-1, model_width)]
    all_to_all x1 -> x0, starting transfers between devices: 5.95 us -> none  [on_device(): lax.all_to_all(expert_out, 'sp', split_axis=0, concat_axis=0, tiled=True)]
    dot_general x1 -> x0, local copies, waits for them, and re-layouts: 5.44 us -> none  [on_device(): jnp.dot(hidden, down_proj[0], preferred_element_type=jnp.float32)]
  transfers between devices with their start and end apart: 2 -> 1, of which waited for: 1 -> 0; matrix products, arithmetic and copies ran while one was open for 2% -> 5% of each run, Pallas kernels for 0% -> 0%
where the time goes in v1:
time: 94.1 us; the launch traced here: 93.6 us
  Pallas kernels  68.4 us (73%)
  local copies, waits for them, and re-layouts  7.46 us (8%)
  blocking collectives  6.31 us (7%)
  other arithmetic  4.89 us (5%)
  starting transfers between devices  3.5 us (4%)
  matrix products  2.97 us (3%)
    pallas_call x1, Pallas kernels, moe(): pl.pallas_call(moe_kernel, out_shape=jax.ShapeDtypeStruct((ROWS, D), BF16...  68.4 us
    all_to_all x1, blocking collectives, summed_on_arrival(): tiles = lax.all_to_all(in_blocks(shard, dim, size), axis, 0, 0, tiled=True)  6.31 us
    unnamed x10, local copies, waits for them, and re-layouts  5.79 us
    ppermute x1, starting transfers between devices, from_behind(): return lax.ppermute(block, axis, route)  3.5 us
    add x1, other arithmetic, on_device(): mixed = residual.astype(jnp.float32) + projected  2.14 us
  transfers between devices with their start and end apart: 1, of which 0 were waited for; matrix products, arithmetic and copies ran while one was open for 5% of the time, Pallas kernels for 0%

profile of v1, /device:TPU:0, one launch (start us, length us, event | category | flops | bytes accessed | tf_op | source)
XLA Modules:
  0.0 93.6 jit_solution(12608730436074789458)
XLA Ops:
  0.0 0.0 copy-start
  0.0 0.0 copy-start.2
  0.0 0.9 slice.12
  0.9 0.7 slice.13
  1.6 3.5 %collective-permute-start = (bf16[128,128]{0,1:T(8,128)(2,1)S(1)}, bf16[128,128]{0,1:T(8,128)(2,1)S(1)}, u32[]{:S(2)}, u32[]{:S(2)}) collective-permute-start(bf16[128,128]{0,1:T(8,128)(2,1)S(1)} %pad_maximum_fusion), channel_id=1, source_target_pairs={{0,2},{2,4},{4,6},{6,8},{8,10},{10,12},{12,14},{14,16},{16,18},{18... | collective-permute-start | bytes 98312 | tf_op jit(solution)/shard_map/ppermute | solution.py:36
  5.2 0.1 subtract_convert_fusion
  5.3 0.2 fusion.13
  5.5 1.1 %copy.18 = bf16[256,512]{0,1:T(8,128)(2,1)S(1)} copy(bf16[256,512]{1,0:T(8,128)(2,1)} %param.12) | data formatting | bytes 524288 | tf_op args[0]
  6.6 1.4 %copy.21.routes_ref = s32[128,2]{1,0:T(8,128)} copy(s32[128,2]{0,1:T(2,128)} %param.19) | data formatting | bytes 2048 | tf_op args[7]
  8.0 1.4 %copy.22.rw_ref = f32[128,2]{1,0:T(8,128)} copy(f32[128,2]{0,1:T(2,128)} %param.20) | data formatting | bytes 2048 | tf_op args[8]
  9.4 0.0 collective-permute-done
  9.4 0.0 copy-start.1
  9.4 1.6 %fusion.22 = (f32[8,256]{1,0:T(8,128)S(1)}, f32[1,8,256,384]{2,3,1,0:T(8,128)S(1)}) fusion(f32[256,384]{0,1:T(8,128)S(1)} %subtract_convert_fusion, f32[8]{0:T(128)S(1)} %multiply_exponential_fusion, bf16[256,8,64]{0,2,1:T(8,128)(2,1)S(1)} %bitcast.35, bf16[256,64]{0,1:T(8,128)(2,1)} %param.13, bf16[128,64]{0,1:T(8,128)(2,1)S(1)} %get-tuple-element.6, ...), kind=kOutput, calls=%fused_computation.34 | convolution fusion | flops 104691712 | bytes 3956768 | tf_op jit(solution)/shard_map/rjwh,cjh->jwrc/dot_general | solution.py:400
  11.0 0.0 copy-done.2
  11.0 0.1 broadcast_maximum_fusion
  11.1 0.4 fusion.1
  11.5 0.1 exponential_add_fusion
  11.6 0.0 copy-done.1
  11.6 0.7 fusion.9
  12.3 0.1 convert_element_type.40
  12.3 0.0 copy-done
  12.4 0.7 fusion.2
  13.1 6.3 %all_to_all.5 = f32[2,128,2048]{2,1,0:T(8,128)} all-to-all(f32[2,128,2048]{2,1,0:T(8,128)S(1)} %fusion.2), channel_id=1, replica_groups=mesh['sp'=64,'tp'=2] {'tp'}, dimensions={0} | all-to-all | bytes 4194304 | tf_op jit(solution)/shard_map/all_to_all | solution.py:46
  19.4 1.8 %reduce_sum.19 = f32[128,2048]{1,0:T(8,128)S(1)} reduce(f32[2,128,2048]{2,1,0:T(8,128)} %all_to_all.5, f32[]{:T(128)} %constant.34.clone.1), dimensions={0}, to_apply=%region_2.3 | reduce | flops 262144 | bytes 3145732 | tf_op jit(solution)/shard_map/reduce_sum | solution.py:47
  21.2 2.1 %convert_add_fusion.mixed_ref = f32[128,2048]{1,0:T(8,128)} fusion(f32[128,2048]{1,0:T(8,128)S(1)} %reduce_sum.19, bf16[128,2048]{1,0:T(8,128)(2,1)} %param.17), kind=kLoop, calls=%fused_computation.11 | loop fusion | flops 524288 | bytes 2621440 | tf_op jit(solution)/shard_map/add | solution.py:436
  23.4 68.4 %moe.1 = bf16[128,2048]{1,0:T(8,128)(2,1)} custom-call(f32[128,2048]{1,0:T(8,128)} %convert_add_fusion.mixed_ref, f32[1,2048]{1,0:T(1,128)} %bitcast.36, s32[128,2]{1,0:T(8,128)} %copy.21.routes_ref, f32[128,2]{1,0:T(8,128)} %copy.22.rw_ref, bf16[1,2048,1792]{2,1,0:T(8,128)(2,1)} %wg_hbm.1, bf16[1,2048,1792]{2,1,0:T(8,128)(2,1)} %wu_hbm.1, ...), custom_call_target="tpu_custom_call" | custom-call | tf_op jit(solution)/shard_map/moe/pallas_call | solution.py:335
  91.7 1.9 %copy.27 = bf16[128,2048]{1,0:T(8,128)(2,1)} copy(bf16[128,2048]{1,0:T(8,128)(2,1)} %moe.1) | data formatting | bytes 1048576
  (6 shorter events, 0.0 us)
Async XLA Ops:
  0.0 12.3 %copy-start = (bf16[512,2048]{1,0:T(8,128)(2,1)S(1)}, bf16[512,2048]{1,0:T(8,128)(2,1)}, u32[]{:S(2)}) copy-start(bf16[512,2048]{1,0:T(8,128)(2,1)} %param.16) | copy-start | bytes 6291460
  0.0 11.0 %copy-start.2 = (f32[8]{0:T(128)S(1)}, f32[8]{0:T(128)}, u32[]{:S(2)}) copy-start(f32[8]{0:T(128)} %param.15) | copy-start | bytes 100
  1.6 7.8 %collective-permute-start = (bf16[128,128]{0,1:T(8,128)(2,1)S(1)}, bf16[128,128]{0,1:T(8,128)(2,1)S(1)}, u32[]{:S(2)}, u32[]{:S(2)}) collective-permute-start(bf16[128,128]{0,1:T(8,128)(2,1)S(1)} %pad_maximum_fusion), channel_id=1, source_target_pairs={{0,2},{2,4},{4,6},{6,8},{8,10},{10,12},{12,14},{14,16},{16,18},{18... | collective-permute-start | bytes 98312 | tf_op jit(solution)/shard_map/ppermute | solution.py:36
  9.4 2.2 %copy-start.1 = (bf16[256,64]{0,1:T(8,128)(2,1)S(1)}, bf16[256,64]{0,1:T(8,128)(2,1)}, u32[]{:S(2)}) copy-start(bf16[256,64]{0,1:T(8,128)(2,1)} %param.14) | copy-start | bytes 98308

commit v2 on v1

v2 whole, which is shorter than its diff:
```python
import jax
import jax.numpy as jnp
from jax import lax
from jax.experimental import pallas as pl
from jax.experimental.pallas import tpu as pltpu
from jax.sharding import PartitionSpec as P

MESH = pl.DeviceIdType.MESH
F32 = jnp.float32
BF16 = jnp.bfloat16

HEADS = 8
HEAD_SIZE = 64
KEYS = 128
ROWS = 128
D = 2048
FFH = 1792
CAP = 6
Q = 4
W = D // Q
BLK = Q * CAP
CH = 4
PER = 16
GB = 8
GR = GB * CAP


def offset_chunks():
    def hops(o):
        return sum(min(v, 4 - v) for v in o)

    def opposite(o):
        return tuple((4 - v) % 4 for v in o)

    every = [(a, b, c) for a in range(4) for b in range(4) for c in range(4)]
    by = {h: [o for o in every if hops(o) == h] for h in range(7)}
    axial = [o for o in by[2] if 2 in o]
    same = [o for o in by[2] if 2 not in o and len(set(v for v in o if v)) == 1]
    mixed = [o for o in by[2] if 2 not in o and o not in same]
    corners = [o for o in by[3] if 2 not in o]
    sides = [o for o in by[3] if 2 in o]
    first = by[0] + by[1] + axial + same
    last = corners + sides[:1] + [opposite(sides[0])] + mixed
    rest = [o for o in by[6] + by[5] + by[4] + by[3] if o not in last]
    middle = [[], []]
    done = set()
    for o in rest:
        if o in done:
            continue
        pair = [o] if opposite(o) == o else [o, opposite(o)]
        done.update(pair)
        middle[0 if len(middle[0]) <= len(middle[1]) else 1] += pair
    while len(middle[0]) > PER:
        middle[1].append(middle[0].pop())
    while len(middle[1]) > PER:
        middle[0].append(middle[1].pop())
    return [first, middle[0], middle[1], last]


CHUNKS = offset_chunks()


def fiota(shape, dim):
    return lax.broadcasted_iota(jnp.int32, shape, dim).astype(F32)


def fdiv(v, n):
    return jnp.floor((v + 0.5) * (1.0 / n))


def layer_kernel(
    q_ref,
    kt_ref,
    vt_ref,
    sink_ref,
    gain_ref,
    routes_ref,
    rw_ref,
    wo_hbm,
    res_hbm,
    wg_hbm,
    wu_hbm,
    wd_hbm,
    out_ref,
    wo,
    res,
    wg,
    wu,
    wd,
    halo,
    kk,
    vv,
    att,
    pj,
    pjr,
    nrm,
    onehot,
    comb_hi,
    comb_lo,
    sbuf,
    mine,
    other,
    xbuf,
    hid,
    pm,
    po,
    pr,
    ysend,
    zbuf,
    acc,
    osem,
    wsem,
    hsend,
    hrecv,
    jsend,
    jrecv,
    dsend,
    drecv,
    fsend,
    frecv,
    psend,
    precv,
    rsend,
    rrecv,
):
    sp = lax.axis_index("sp")
    tp = lax.axis_index("tp")
    x, y, z = sp % 4, (sp // 4) % 4, sp // 16
    partner = (sp, 1 - tp)

    barrier = pltpu.get_barrier_semaphore()

    def greet(i, _):
        pl.semaphore_signal(barrier, inc=1, device_id=((sp + i) % 64, tp), device_id_type=MESH)
        return 0

    lax.fori_loop(1, 64, greet, 0)
    pl.semaphore_signal(barrier, inc=1, device_id=partner, device_id_type=MESH)

    ocopies = [
        pltpu.make_async_copy(wo_hbm, wo, osem.at[0]),
        pltpu.make_async_copy(res_hbm, res, osem.at[1]),
    ]
    for c in ocopies:
        c.start()
    wcopies = []
    for k, (src, dst) in enumerate(((wg_hbm, wg), (wu_hbm, wu), (wd_hbm, wd))):
        part = src.shape[1] // 4
        for j in range(4):
            rows = pl.ds(j * part, part)
            wcopies.append(pltpu.make_async_copy(src.at[0, rows], dst.at[rows], wsem.at[k, j]))

    qi, kc = fiota((KEYS, 2 * KEYS), 0), fiota((KEYS, 2 * KEYS), 1)
    dist = qi + KEYS - kc
    window = (dist >= 0.0) & (dist < KEYS)
    tier = jnp.where(tp == 0, 1.0, 2.0 ** (-HEADS / 2)).astype(F32)
    first = jnp.where(sp == 0, float(KEYS), 0.0).astype(F32)
    kk[...] = jnp.zeros_like(kk)
    vv[...] = jnp.zeros_like(vv)

    def attend(b):
        for ref, own, n in ((kk, kt_ref, 0), (vv, vt_ref, 1)):
            for h in range(2):
                rows = slice(h * HEAD_SIZE, (h + 1) * HEAD_SIZE)
                lane = h * 2 * KEYS
                if b == 1:
                    ref[rows, lane : lane + 2 * KEYS] = own[...]
                else:
                    ref[rows, lane : lane + KEYS] = halo[n]
                    ref[rows, lane + KEYS : lane + 2 * KEYS] = own[:, :KEYS]
        seen = window if b == 1 else window & (kc >= first)
        far = jnp.where(seen, dist, jnp.inf)
        rows = slice(b * KEYS, (b + 1) * KEYS)
        for p in range(HEADS // 2):
            lanes = slice(p * 2 * HEAD_SIZE, (p + 1) * 2 * HEAD_SIZE)
            score = jnp.dot(q_ref[rows, lanes], kk[...], preferred_element_type=F32)
            probs = []
            for h in range(2):
                j = 2 * p + h
                one = score[:, h * 2 * KEYS : (h + 1) * 2 * KEYS] * HEAD_SIZE**-0.5
                one = one - far * (tier * 2.0 ** (-(j + 1) / 2))
                sink = jnp.broadcast_to(sink_ref[0:1, j : j + 1], (KEYS, 1))
                peak = jnp.maximum(jnp.max(one, axis=-1, keepdims=True), sink)
                e = jnp.exp(one - peak)
                denom = jnp.sum(e, axis=-1, keepdims=True) + jnp.exp(sink - peak)
                probs.append((e * (1.0 / denom)).astype(BF16))
            both = jnp.concatenate(probs, axis=1)
            o = lax.dot_general(
                both, vv[...], (((1,), (1,)), ((), ())), preferred_element_type=F32
            )
            att[rows, lanes] = o.astype(BF16)

    def piece(k):
        cols = slice(k * W, (k + 1) * W)
        return pltpu.make_async_remote_copy(
            src_ref=pj.at[1 - tp, :, cols],
            dst_ref=pjr.at[:, cols],
            send_sem=jsend.at[k],
            recv_sem=jrecv.at[k],
            device_id=partner,
            device_id_type=MESH,
        )

    def project(b):
        rows = slice(b * KEYS, (b + 1) * KEYS)
        for k in range(Q):
            cols = slice(k * W, (k + 1) * W)
            pj[b, :, cols] = jnp.dot(att[rows], wo[:, cols], preferred_element_type=F32)
            if b == 0:
                piece(k).start()

    def spots(g):
        return [
            ((z + dz) % 4) * 16 + ((y + dy) % 4) * 4 + (x + dx) % 4 for dx, dy, dz in CHUNKS[g]
        ]

    def sources(g):
        return [
            ((z + 4 - dz) % 4) * 16 + ((y + 4 - dy) % 4) * 4 + (x + 4 - dx) % 4
            for dx, dy, dz in CHUNKS[g]
        ]

    r0, r1 = routes_ref[0:1, :], routes_ref[1:2, :]
    ri, ci = fiota((ROWS, ROWS), 0), fiota((ROWS, ROWS), 1)
    eye = jnp.where(ri == ci, 1.0, 0.0)
    br = fiota((BLK, ROWS), 0)
    bq = fdiv(br, CAP)
    bs = br - bq * CAP

    def select(g):
        upper = jnp.where(ri < ci, 1.0, 0.0).astype(BF16)
        row = lax.broadcasted_iota(jnp.int32, (PER, ROWS), 0)
        e = jnp.zeros((PER, ROWS), jnp.int32)
        for i, spot in enumerate(spots(g)):
            e = jnp.where(row == i, spot, e)
        cnt = jnp.where((e == r0) | (e == r1), 1.0, 0.0)
        rank = jnp.dot(cnt.astype(BF16), upper, preferred_element_type=F32)
        code = jnp.where(cnt > 0.0, rank, -1.0)
        code = jnp.broadcast_to(code[:, None, :], (PER, BLK, ROWS))
        for k in range(Q):
            want = jnp.where(bq == k, bs, -2.0)
            hit = jnp.where(code == want[None], 1.0, 0.0).reshape(PER * BLK, ROWS)
            onehot[g, :, k * ROWS : (k + 1) * ROWS] = hit.astype(BF16)

    def column(v):
        return jnp.sum(eye * v.astype(F32), axis=1, keepdims=True)

    def weigh(g, c0, c1, w0, w1):
        lower = jnp.where(ci < ri, 1.0, 0.0).astype(BF16)
        lane = fiota((8, PER * BLK), 1)
        i = fdiv(lane, BLK)
        quarter = fdiv(lane - i * BLK, CAP)
        slot = (lane - i * BLK - quarter * CAP)[0:1]
        e = jnp.zeros((8, PER * BLK), F32)
        for n, spot in enumerate(spots(g)):
            e = jnp.where(i == n, spot.astype(F32), e)
        e = e[0:1]
        quarter = quarter[0:1]
        is0, is1 = e == c0, e == c1
        cnt = jnp.where(is0 | is1, 1.0, 0.0)
        rank = jnp.dot(lower, cnt.astype(BF16), preferred_element_type=F32)
        wt = jnp.where(is0, w0, 0.0) + jnp.where(is1, w1, 0.0)
        wt = jnp.where(rank == slot, wt, 0.0)
        hi = wt.astype(BF16).astype(F32)
        lo = wt - hi
        for k in range(Q):
            rows = slice(k * ROWS, (k + 1) * ROWS)
            comb_hi[g, rows] = jnp.where(quarter == k, hi, 0.0).astype(BF16)
            comb_lo[g, rows] = jnp.where(quarter == k, lo, 0.0).astype(BF16)

    def lo_of(g):
        return 1 if g == 0 else 0

    def exchange(g, src, dst, ssem, rsem, peers):
        for i in range(lo_of(g), PER):
            pltpu.make_async_remote_copy(
                src_ref=src.at[g * PER + i],
                dst_ref=dst.at[g * PER + i],
                send_sem=ssem.at[g],
                recv_sem=rsem.at[g],
                device_id=(peers[i], tp),
                device_id_type=MESH,
            ).start()

    def whole(g, src, dst, ssem, rsem):
        rows = pl.ds(g * PER + lo_of(g), PER - lo_of(g))
        return pltpu.make_async_remote_copy(
            src_ref=src.at[rows],
            dst_ref=dst.at[rows],
            send_sem=ssem.at[g],
            recv_sem=rsem.at[g],
            device_id=partner,
            device_id_type=MESH,
        )

    def forward(g):
        rows = pl.ds(g * PER, PER)
        return pltpu.make_async_remote_copy(
            src_ref=mine.at[rows],
            dst_ref=other.at[rows],
            send_sem=fsend.at[g],
            recv_sem=frecv.at[g],
            device_id=partner,
            device_id_type=MESH,
        )

    def swap(g, h):
        return pltpu.make_async_remote_copy(
            src_ref=po.at[g, h],
            dst_ref=pr.at[g, h],
            send_sem=psend.at[g, h],
            recv_sem=precv.at[g, h],
            device_id=partner,
            device_id_type=MESH,
        )

    def dispatch(g):
        rows = jnp.dot(onehot[g], nrm[...], preferred_element_type=F32).astype(BF16)
        rows = rows.reshape(PER, BLK, W)
        sbuf[pl.ds(g * PER, PER)] = rows
        if g == 0:
            mine[0] = rows[0]

    def send(g):
        exchange(g, sbuf, mine, dsend, drecv, spots(g))

    def permutation(inverse):
        pi, pj_ = fiota((GB * BLK, GB * BLK), 0), fiota((GB * BLK, GB * BLK), 1)
        a, b = (pj_, pi) if inverse else (pi, pj_)
        iq = fdiv(a, GR)
        ib = fdiv(a - iq * GR, CAP)
        ist = a - iq * GR - ib * CAP
        return jnp.where(ib * BLK + iq * CAP + ist == b, 1.0, 0.0).astype(BF16)

    def spread(g):
        unpack = permutation(False)
        for h in range(4):
            src = mine if h < 2 else other
            blocks = src[pl.ds(g * PER + (h % 2) * GB, GB)].reshape(GB * BLK, W)
            rows = jnp.dot(unpack, blocks, preferred_element_type=F32).astype(BF16)
            for q in range(Q):
                xbuf[h * GR : (h + 1) * GR, q * W : (q + 1) * W] = rows[q * GR : (q + 1) * GR]

    def gate_up(tiles):
        for k in tiles:
            cols = slice(k * 256, (k + 1) * 256)
            a = jnp.dot(xbuf[...], wg[:, cols], preferred_element_type=F32)
            b = jnp.dot(xbuf[...], wu[:, cols], preferred_element_type=F32)
            hid[:, cols] = (a / (1.0 + jnp.exp(-a)) * b).astype(BF16)

    def down(g):
        for k in range(Q):
            cols = slice(k * W, (k + 1) * W)
            a = jnp.dot(hid[...], wd[:, cols], preferred_element_type=F32).astype(BF16)
            pm[g % 2, :, cols] = a[: 2 * GR]
            po[g, k // 2, :, (k % 2) * W : (k % 2 + 1) * W] = a[2 * GR :]
            if k % 2 == 1:
                swap(g, k // 2).start()

    def give_back(g):
        pack = permutation(True)
        swap(g, 0).wait_recv()
        swap(g, 1).wait_recv()
        for h in range(2):
            rows = slice(h * GR, (h + 1) * GR)
            stack = []
            for k in range(Q):
                a = pm[g % 2, rows, k * W : (k + 1) * W].astype(F32)
                b = pr[g, k // 2, rows, (k % 2) * W : (k % 2 + 1) * W].astype(F32)
                stack.append((a + b).astype(BF16))
            packed = jnp.dot(pack, jnp.concatenate(stack, axis=0), preferred_element_type=F32)
            packed = packed.astype(BF16).reshape(GB, BLK, W)
            ysend[pl.ds(g * PER + h * GB, GB)] = packed
            if g == 0 and h == 0:
                zbuf[0] = packed[0]
        exchange(g, ysend, zbuf, rsend, rrecv, sources(g))

    def combine(g):
        whole(g, ysend, zbuf, rsend, rrecv).wait_recv()
        back = zbuf[pl.ds(g * PER, PER)].reshape(PER * BLK, W)
        both = jnp.dot(comb_hi[g], back, preferred_element_type=F32) + jnp.dot(
            comb_lo[g], back, preferred_element_type=F32
        )
        if g + 1 < CH:
            acc[...] += both
        else:
            total = (acc[...] + both).astype(BF16)
            for k in range(Q):
                out_ref[:, k * W : (k + 1) * W] = total[k * ROWS : (k + 1) * ROWS]

    attend(1)
    for c in ocopies:
        c.wait()
    for c in wcopies:
        c.start()
    project(1)
    for g in range(CH):
        select(g)
    pl.semaphore_wait(barrier, 64)
    whole_halo = pltpu.make_async_remote_copy(
        src_ref=halo,
        dst_ref=halo,
        send_sem=hsend,
        recv_sem=hrecv,
        device_id=((sp + 1) % 64, tp),
        device_id_type=MESH,
    )

    @pl.when(sp < 63)
    def _():
        for n, ref in enumerate((kt_ref, vt_ref)):
            pltpu.make_async_remote_copy(
                src_ref=ref.at[:, KEYS:],
                dst_ref=halo.at[n],
                send_sem=hsend,
                recv_sem=hrecv,
                device_id=((sp + 1) % 64, tp),
                device_id_type=MESH,
            ).start()

    wcol = [column(v) for v in (r0, r1, rw_ref[0:1, :], rw_ref[1:2, :])]
    for g in range(CH):
        weigh(g, *wcol)

    @pl.when(sp == 0)
    def _():
        halo[...] = jnp.zeros_like(halo)

    @pl.when(sp > 0)
    def _():
        whole_halo.wait_recv()

    attend(0)
    project(0)

    total = jnp.zeros((ROWS, 1), F32)
    for k in range(Q):
        piece(k).wait_recv()
        cols = slice(k * W, (k + 1) * W)
        m = res[:, cols].astype(F32) + (pj[tp, :, cols] + pjr[:, cols])
        acc[k * ROWS : (k + 1) * ROWS, :] = m
        total = total + jnp.sum(m * m, axis=-1, keepdims=True)
    scale = lax.rsqrt(total * (1.0 / D) + 1e-05)
    for k in range(Q):
        rows = slice(k * ROWS, (k + 1) * ROWS)
        gain = gain_ref[:, k * W : (k + 1) * W]
        nrm[rows] = (acc[rows] * scale * gain).astype(BF16)
    dispatch(0)
    send(0)
    dispatch(1)
    whole(0, sbuf, mine, dsend, drecv).wait_send()
    send(1)
    dispatch(2)
    dispatch(3)
    whole(0, sbuf, mine, dsend, drecv).wait_recv()
    forward(0).start()
    for c in wcopies:
        c.wait()
    for g in range(CH):
        forward(g).wait_recv()
        spread(g)
        gate_up(range(3))
        if g == 0:
            send(2)
        if g > 0:
            give_back(g - 1)
        gate_up(range(3, FFH // 256))
        if g == 0:
            send(3)
        if g + 1 < CH:
            whole(g + 1, sbuf, mine, dsend, drecv).wait_recv()
            forward(g + 1).start()
        down(g)
    give_back(CH - 1)
    for g in range(CH):
        combine(g)

    @pl.when(sp < 63)
    def _():
        whole_halo.wait_send()

    for k in range(Q):
        piece(k).wait_send()
    for g in range(CH):
        if g > 0:
            whole(g, sbuf, mine, dsend, drecv).wait_send()
        forward(g).wait_send()
        swap(g, 0).wait_send()
        swap(g, 1).wait_send()
        whole(g, ysend, zbuf, rsend, rrecv).wait_send()


def on_device(
    query_rows,
    key_rows,
    value_head_rows,
    sink_logit_head,
    out_weight,
    residual,
    norm_gain,
    routes,
    route_weights,
    gate_proj,
    up_proj,
    down_proj,
):
    vm = pl.BlockSpec(memory_space=pltpu.VMEM)
    hbm = pl.BlockSpec(memory_space=pl.ANY)
    sem = pltpu.SemaphoreType.DMA
    blocks = pltpu.VMEM((CH * PER, BLK, W), BF16)
    return pl.pallas_call(
        layer_kernel,
        out_shape=jax.ShapeDtypeStruct((ROWS, D), BF16),
        in_specs=[vm] * 7 + [hbm] * 5,
        out_specs=vm,
        scratch_shapes=[
            pltpu.VMEM((HEADS * HEAD_SIZE, D), BF16),
            pltpu.VMEM((ROWS, D), BF16),
            pltpu.VMEM((D, FFH), BF16),
            pltpu.VMEM((D, FFH), BF16),
            pltpu.VMEM((FFH, D), BF16),
            pltpu.VMEM((2, HEAD_SIZE, KEYS), BF16),
            pltpu.VMEM((2 * HEAD_SIZE, 4 * KEYS), BF16),
            pltpu.VMEM((2 * HEAD_SIZE, 4 * KEYS), BF16),
            pltpu.VMEM((2 * KEYS, HEADS * HEAD_SIZE), BF16),
            pltpu.VMEM((2, ROWS, D), F32),
            pltpu.VMEM((ROWS, D), F32),
            pltpu.VMEM((Q * ROWS, W), BF16),
            pltpu.VMEM((CH, PER * BLK, Q * ROWS), BF16),
            pltpu.VMEM((CH, Q * ROWS, PER * BLK), BF16),
            pltpu.VMEM((CH, Q * ROWS, PER * BLK), BF16),
            blocks,
            blocks,
            blocks,
            pltpu.VMEM((4 * GR, D), BF16),
            pltpu.VMEM((4 * GR, FFH), BF16),
            pltpu.VMEM((2, 2 * GR, D), BF16),
            pltpu.VMEM((CH, 2, 2 * GR, D // 2), BF16),
            pltpu.VMEM((CH, 2, 2 * GR, D // 2), BF16),
            blocks,
            blocks,
            pltpu.VMEM((Q * ROWS, W), F32),
            sem((2,)),
            sem((3, 4)),
            sem,
            sem,
            sem((Q,)),
            sem((Q,)),
            sem((CH,)),
            sem((CH,)),
            sem((CH,)),
            sem((CH,)),
            sem((CH, 2)),
            sem((CH, 2)),
            sem((CH,)),
            sem((CH,)),
        ],
        compiler_params=pltpu.CompilerParams(
            collective_id=0, has_side_effects=True, vmem_limit_bytes=60 * 1024 * 1024
        ),
        name="layer",
    )(
        query_rows,
        key_rows.T,
        value_head_rows.T,
        sink_logit_head.reshape(1, HEADS),
        norm_gain.reshape(1, D),
        routes.T,
        route_weights.T,
        out_weight,
        residual,
        gate_proj,
        up_proj,
        down_proj,
    )


def solution(mesh):
    placed = (
        P("sp", "tp"),
        P("sp", "tp"),
        P("sp", "tp"),
        P("tp"),
        P("tp", None),
        P(("sp", "tp"), None),
        P(),
        P(("sp", "tp"), None),
        P(("sp", "tp"), None),
        P("sp", None, "tp"),
        P("sp", None, "tp"),
        P("sp", "tp", None),
    )
    return jax.shard_map(
        on_device, mesh=mesh, in_specs=placed, out_specs=P(("sp", "tp"), None), check_vma=False
    )
```

time: 94.1 us -> 71.2 us (0.76)
  blocking collectives: 6.31 us -> 0 us
  local copies, waits for them, and re-layouts: 7.46 us -> 1.88 us
  other arithmetic: 4.89 us -> 0 us
  starting transfers between devices: 3.5 us -> 0 us
  matrix products: 2.97 us -> 0 us
    all_to_all x1 -> x0, blocking collectives: 6.31 us -> none  [summed_on_arrival(): tiles = lax.all_to_all(in_blocks(shard, dim, size), axis, 0, 0, tiled=True)]
    unnamed x10 -> x1, local copies, waits for them, and re-layouts: 5.79 us -> 1.88 us
    ppermute x1 -> x0, starting transfers between devices: 3.5 us -> none  [from_behind(): return lax.ppermute(block, axis, route)]
    dot_general x3 -> x0, matrix products: 2.97 us -> none  [the longest x1 1.55 us: on_device(): jnp.einsum('rjwh,cjh->jwrc', query_rows.reshape(length, local_kv, query_g...]
    reduce_sum x2 -> x0, other arithmetic: 2.28 us -> none  [the longest x1 1.84 us: summed_on_arrival(): return jnp.sum(tiles, axis=0)]
    add x4 -> x0, other arithmetic: 2.23 us -> none  [the longest x1 2.14 us: on_device(): mixed = residual.astype(jnp.float32) + projected]
    slice x3 -> x0, local copies, waits for them, and re-layouts: 1.6 us -> none  [the longest x1 0.88 us: on_device(): key_rows[length - WINDOW_KEYS:]]
  transfers between devices with their start and end apart: 1 -> 0, of which waited for: 0 -> 0; matrix products, arithmetic and copies ran while one was open for 5% -> 0% of each run, Pallas kernels for 0% -> 0%
where the time goes in v2:
time: 71.2 us; the launch traced here: 70.1 us
  Pallas kernels  68.2 us (96%)
  local copies, waits for them, and re-layouts  1.88 us (3%)
    pallas_call x1, Pallas kernels, on_device(): pl.pallas_call(layer_kernel, out_shape=jax.ShapeDtypeStruct((ROWS, D), BF...  68.2 us
    unnamed x1, local copies, waits for them, and re-layouts  1.88 us

profile of v2, /device:TPU:0, one launch (start us, length us, event | category | flops | bytes accessed | tf_op | source)
XLA Modules:
  0.0 70.1 jit_solution(10241095016197636835)
XLA Ops:
  0.0 68.2 %layer.1 = bf16[128,2048]{1,0:T(8,128)(2,1)} custom-call(bf16[256,512]{1,0:T(8,128)(2,1)} %q_ref.1, bf16[64,256]{1,0:T(8,128)(2,1)} %bitcast.6, bf16[64,256]{1,0:T(8,128)(2,1)} %bitcast.7, f32[1,8]{1,0:T(1,128)} %bitcast.11, f32[1,2048]{1,0:T(1,128)} %bitcast.8, s32[2,128]{1,0:T(2,128)} %bitcast.9, f32[2,128]{1,0:T(2,128)} %bitcast.10, ...), custom_call_target="tpu_custom_call" | custom-call | tf_op jit(solution)/shard_map/layer/pallas_call | solution.py:511
  68.2 1.9 %copy.14 = bf16[128,2048]{1,0:T(8,128)(2,1)} copy(bf16[128,2048]{1,0:T(8,128)(2,1)} %layer.1) | data formatting | bytes 1048576

commit v3 on v2

--- a/solution.py
+++ b/solution.py
@@ -42,19 +42,8 @@
     first = by[0] + by[1] + axial + same
     last = corners + sides[:1] + [opposite(sides[0])] + mixed
     rest = [o for o in by[6] + by[5] + by[4] + by[3] if o not in last]
-    middle = [[], []]
-    done = set()
-    for o in rest:
-        if o in done:
-            continue
-        pair = [o] if opposite(o) == o else [o, opposite(o)]
-        done.update(pair)
-        middle[0 if len(middle[0]) <= len(middle[1]) else 1] += pair
-    while len(middle[0]) > PER:
-        middle[1].append(middle[0].pop())
-    while len(middle[1]) > PER:
-        middle[0].append(middle[1].pop())
-    return [first, middle[0], middle[1], last]
+    rest.sort(key=hops, reverse=True)
+    return [first, rest[:PER], rest[PER:], last]
 
 
 CHUNKS = offset_chunks()
@@ -454,19 +443,18 @@
     dispatch(3)
     whole(0, sbuf, mine, dsend, drecv).wait_recv()
     forward(0).start()
+    send(2)
     for c in wcopies:
         c.wait()
     for g in range(CH):
         forward(g).wait_recv()
         spread(g)
-        gate_up(range(3))
+        gate_up(range(2))
         if g == 0:
-            send(2)
+            send(3)
         if g > 0:
             give_back(g - 1)
-        gate_up(range(3, FFH // 256))
-        if g == 0:
-            send(3)
+        gate_up(range(2, FFH // 256))
         if g + 1 < CH:
             whole(g + 1, sbuf, mine, dsend, drecv).wait_recv()
             forward(g + 1).start()

time: 71.2 us -> 68.2 us (0.958)
  Pallas kernels: 68.2 us -> 65.5 us
    pallas_call x1, Pallas kernels: 68.2 us -> 65.5 us  [on_device(): pl.pallas_call(layer_kernel, out_shape=jax.ShapeDtypeStruct((ROWS, D), BF...]
where the time goes in v3:
time: 68.2 us; the launch traced here: 67.4 us
  Pallas kernels  65.5 us (96%)
  local copies, waits for them, and re-layouts  1.88 us (3%)
    pallas_call x1, Pallas kernels, on_device(): pl.pallas_call(layer_kernel, out_shape=jax.ShapeDtypeStruct((ROWS, D), BF...  65.5 us
    unnamed x1, local copies, waits for them, and re-layouts  1.88 us

profile of v3, /device:TPU:0, one launch (start us, length us, event | category | flops | bytes accessed | tf_op | source)
XLA Modules:
  0.0 67.4 jit_solution(2453229581002675828)
XLA Ops:
  0.0 65.5 %layer.1 = bf16[128,2048]{1,0:T(8,128)(2,1)} custom-call(bf16[256,512]{1,0:T(8,128)(2,1)} %q_ref.1, bf16[64,256]{1,0:T(8,128)(2,1)} %bitcast.6, bf16[64,256]{1,0:T(8,128)(2,1)} %bitcast.7, f32[1,8]{1,0:T(1,128)} %bitcast.11, f32[1,2048]{1,0:T(1,128)} %bitcast.8, s32[2,128]{1,0:T(2,128)} %bitcast.9, f32[2,128]{1,0:T(2,128)} %bitcast.10, ...), custom_call_target="tpu_custom_call" | custom-call | tf_op jit(solution)/shard_map/layer/pallas_call | solution.py:499
  65.5 1.9 %copy.14 = bf16[128,2048]{1,0:T(8,128)(2,1)} copy(bf16[128,2048]{1,0:T(8,128)(2,1)} %layer.1) | data formatting | bytes 1048576
